TPU v7x, 32 devices: a whole 2x2x4 slice. The times are simulated.
32 devices in a mesh: rep: 2 (over x), fs: 4 (over z), tp: 4 (over y, core).
Axes of the slice: x: 2, y: 2, z: 4, core: 2. Of those that a mesh axis runs over, the one named last changes fastest.
Arguments:
- tokens: bfloat16 [1024, 4096], P(('rep', 'fs'), 'tp'), may hold values from -6 to 6
- mixer_gain: float32 [4096], replicated, may hold values from 0.75 to 1.25
- gate_proj: bfloat16 [4096, 2048], P('fs', 'tp'), may hold values from -0.09375 to 0.09375
- value_proj: bfloat16 [4096, 2048], P('fs', 'tp'), may hold values from -0.09375 to 0.09375
- value_gain: float32 [16, 128], P('tp'), may hold values from 0.75 to 1.25
- spatial_mix: bfloat16 [16, 128, 128], P('tp', 'fs'), may hold values from -0.5 to 0.5
- spatial_bias: float32 [16, 128], P('tp'), may hold values from 0.5 to 1.5
- head_gain: float32 [16, 128], P('tp'), may hold values from 0.75 to 1.25
- merge_proj: bfloat16 [2048, 4096], P('tp', 'fs'), may hold values from -0.125 to 0.125
- ffn_gain: float32 [4096], replicated, may hold values from 0.25 to 1.75
- gate_up: bfloat16 [4096, 11008], P('fs', 'tp'), may hold values from -0.09375 to 0.09375
- value_up: bfloat16 [4096, 11008], P('fs', 'tp'), may hold values from -0.09375 to 0.09375
- gate_kernel: float32 [3, 11008], P(None, 'tp'), may hold values from -3.5 to 3.5
- value_kernel: float32 [3, 11008], P(None, 'tp'), may hold values from -3.5 to 3.5
- gate_offset: float32 [11008], P('tp'), may hold values from -0.6 to 0.6
- value_offset: float32 [11008], P('tp'), may hold values from -1.8 to 1.8
- down_proj: bfloat16 [11008, 4096], P('tp', 'fs'), may hold values from -0.0546875 to 0.0546875
Outputs:
- layer_out: bfloat16 [1024, 4096], P(('rep', 'fs'), 'tp')
All inputs are finite; a program needn't handle non-finite values.
Results may differ from a plain program's by a relative error of at most 0.02.
Values may be sent and summed in bfloat16 or wider, within the bound.
A program may use at most 128 MiB of HBM per device.

v0:
```python
import jax
import jax.numpy as jnp
from jax import lax
from jax.sharding import PartitionSpec as P

epsilon = 1e-06


def over_all(slab, axis, dim, hop, start):
    def gathered(part):
        return lax.all_gather(part, axis, axis=dim, tiled=True)

    return hop(start, jax.tree.map(gathered, slab), jnp.int32(0))


def on_whole(shard, axis, dim, work):
    return work(lax.all_gather(shard, axis, axis=dim, tiled=True), jnp.int32(0))


def normalize(values, gain):
    values = values.astype(jnp.float32)
    scaled = values * lax.rsqrt(jnp.mean(values * values, axis=-1, keepdims=True) + epsilon)
    return scaled * gain


def rounded(values):
    return lax.optimization_barrier(values.astype(jnp.bfloat16)).astype(jnp.float32)


def gelu_exact(values):
    return jax.nn.gelu(values, approximate=False)


def convolve(values, kernel, offset, length):
    total_rows, width = values.shape
    blocks = values.reshape(total_rows // length, length, width)
    padded = jnp.pad(blocks, ((0, 0), (1, 1), (0, 0)))
    result = (
        offset
        + padded[:, 0:length] * kernel[0]
        + padded[:, 1 : length + 1] * kernel[1]
        + padded[:, 2:] * kernel[2]
    )
    return result.reshape(total_rows, width)


def add_block(total, whole, piece, start):
    columns = lax.dynamic_slice_in_dim(whole, start, piece.shape[0], 1)
    return total + jnp.dot(columns, piece, preferred_element_type=jnp.float32)


def on_device(
    tokens,
    mixer_gain,
    gate_proj,
    value_proj,
    value_gain,
    spatial_mix,
    spatial_bias,
    head_gain,
    merge_proj,
    ffn_gain,
    gate_up,
    value_up,
    gate_kernel,
    value_kernel,
    gate_offset,
    value_offset,
    down_proj,
):
    heads_here = spatial_mix.shape[0]
    length = spatial_mix.shape[2]
    whole = lax.all_gather(tokens, "tp", axis=1, tiled=True)
    normed = normalize(whole, mixer_gain).astype(jnp.bfloat16)
    total_rows = normed.shape[0]
    width = gate_proj.shape[1]
    empty = jnp.zeros((total_rows, width), jnp.float32)

    def add_mixer(total, piece, start):
        return add_block(total, normed, piece, start)

    first = over_all(gate_proj, "fs", 0, add_mixer, empty)
    second = over_all(value_proj, "fs", 0, add_mixer, empty)
    gated = gelu_exact(rounded(first))
    spread = gelu_exact(rounded(second))
    head_width = width // heads_here
    seqs = total_rows // length
    spread = normalize(spread.reshape(seqs, length, heads_here, head_width), value_gain).astype(
        jnp.bfloat16
    )
    matrix = lax.all_gather(spatial_mix, "fs", axis=1, tiled=True)
    mixed = jnp.einsum("hij,njhd->nihd", matrix, spread, preferred_element_type=jnp.float32)
    mixed = mixed + spatial_bias.T[None, :, :, None]
    joined = gated.reshape(seqs, length, heads_here, head_width) * mixed
    merged = normalize(joined, head_gain).astype(jnp.bfloat16).reshape(total_rows, width)

    def project_merge(piece, start):
        return jnp.dot(merged, piece, preferred_element_type=jnp.float32)

    merge_terms = on_whole(merge_proj, "fs", 1, project_merge)
    branch = lax.psum_scatter(
        merge_terms.astype(jnp.bfloat16), "tp", scatter_dimension=1, tiled=True
    ).astype(jnp.float32)
    hidden = (tokens.astype(jnp.float32) + branch).astype(jnp.bfloat16)
    full_rows = lax.all_gather(hidden, "tp", axis=1, tiled=True)
    normed_ffn = normalize(full_rows, ffn_gain).astype(jnp.bfloat16)
    inner = gate_up.shape[1]
    blank = jnp.zeros((total_rows, inner), jnp.float32)

    def add_ffn(total, piece, start):
        return add_block(total, normed_ffn, piece, start)

    upper_gate = over_all(gate_up, "fs", 0, add_ffn, blank)
    upper_value = over_all(value_up, "fs", 0, add_ffn, blank)
    conv_gate = convolve(rounded(upper_gate), gate_kernel, gate_offset, length)
    conv_value = convolve(rounded(upper_value), value_kernel, value_offset, length)
    active = (gelu_exact(conv_gate) * conv_value).astype(jnp.bfloat16)

    def project_down(piece, start):
        return jnp.dot(active, piece, preferred_element_type=jnp.float32)

    down_terms = on_whole(down_proj, "fs", 1, project_down)
    change = lax.psum_scatter(
        down_terms.astype(jnp.bfloat16), "tp", scatter_dimension=1, tiled=True
    ).astype(jnp.float32)
    return (hidden.astype(jnp.float32) + change).astype(jnp.bfloat16)


def solution(mesh):
    in_specs = (
        P(("rep", "fs"), "tp"),
        P(),
        P("fs", "tp"),
        P("fs", "tp"),
        P("tp", None),
        P("tp", "fs", None),
        P("tp", None),
        P("tp", None),
        P("tp", "fs"),
        P(),
        P("fs", "tp"),
        P("fs", "tp"),
        P(None, "tp"),
        P(None, "tp"),
        P("tp"),
        P("tp"),
        P("tp", "fs"),
    )
    out_specs = P(("rep", "fs"), "tp")
    return jax.shard_map(
        on_device, mesh=mesh, in_specs=in_specs, out_specs=out_specs, check_vma=False
    )
```

profile of v0, /device:TPU:4, one launch (start us, length us, event | category | flops | bytes accessed | tf_op | source)
XLA Modules:
  0.0 1510.5 jit_solution(930691923512974085)
XLA Ops:
  6.5 0.7 all-gather.9.cloned.1.call-update
  9.4 13.6 all_gather.30
  23.0 2.6 all-gather.9.cloned.1.call-done
  25.6 1.5 fusion
  27.1 81.3 %all-gather.13.cloned.1.call-done = bf16[4096,512]{1,0:T(8,128)(2,1)} async-done(((bf16[1024,512]{1,0:T(8,128)(2,1)}), bf16[4096,512]{1,0:T(8,128)(2,1)}) %all-gather.13.cloned.1.call-update) | async-done | bytes 4194320 | tf_op jit(solution)/shard_map/all_gather | solution.py:11
  108.5 3.3 convolution_convert_fusion.4
  112.9 76.1 %all-gather.11.cloned.1.call-done = bf16[4096,512]{1,0:T(8,128)(2,1)} async-done(((bf16[1024,512]{1,0:T(8,128)(2,1)}), bf16[4096,512]{1,0:T(8,128)(2,1)}) %all-gather.11.cloned.1.call-update) | async-done | bytes 4194320 | tf_op jit(solution)/shard_map/all_gather | solution.py:11
  189.0 2.9 convolution_convert_fusion.5
  193.2 76.3 %all-gather.15.cloned.1.call-done = bf16[512,4096]{1,0:T(8,128)(2,1)} async-done(((bf16[512,1024]{1,0:T(8,128)(2,1)}), bf16[512,4096]{1,0:T(8,128)(2,1)}) %all-gather.15.cloned.1.call-update) | async-done | bytes 4194320 | tf_op jit(solution)/shard_map/all_gather | solution.py:17
  269.4 3.9 convolution_convert_fusion.1
  273.5 22.5 %reduce-scatter.3.cloned.1.call-done = bf16[128,1024]{1,0:T(8,128)(2,1)} async-done(((bf16[128,4096]{1,0:T(8,128)(2,1)}), bf16[128,1024]{1,0:T(8,128)(2,1)}) %reduce-scatter.3.cloned.1.call-update) | async-done | bytes 262160 | tf_op jit(solution)/shard_map/reduce_scatter | solution.py:101
  295.9 1.7 add_convert_fusion.1
  300.4 14.0 all-gather.17.cloned.1.call-done
  314.4 1.6 fusion.3
  316.1 383.5 %all-gather.19.cloned.1.call-done = bf16[4096,2752]{0,1:T(8,128)(2,1)} async-done(((bf16[1024,2752]{0,1:T(8,128)(2,1)}), bf16[4096,2752]{0,1:T(8,128)(2,1)}) %all-gather.19.cloned.1.call-update) | async-done | bytes 22544400 | tf_op jit(solution)/shard_map/all_gather | solution.py:11
  699.6 10.7 convolution_convert_fusion.3
  710.2 371.8 %all-gather.21.cloned.1.call-done = bf16[4096,2752]{0,1:T(8,128)(2,1)} async-done(((bf16[1024,2752]{0,1:T(8,128)(2,1)}), bf16[4096,2752]{0,1:T(8,128)(2,1)}) %all-gather.21.cloned.1.call-update) | async-done | bytes 22544400 | tf_op jit(solution)/shard_map/all_gather | solution.py:11
  1082.0 10.7 convolution_convert_fusion.2
  1092.7 1.3 convert_bitcast_fusion.1
  1094.0 1.2 convert_bitcast_fusion
  1095.2 369.3 %all-gather.23.cloned.1.call-done = bf16[2752,4096]{1,0:T(8,128)(2,1)} async-done(((bf16[2752,1024]{1,0:T(8,128)(2,1)}), bf16[2752,4096]{1,0:T(8,128)(2,1)}) %all-gather.23.cloned.1.call-update) | async-done | bytes 22544400 | tf_op jit(solution)/shard_map/all_gather | solution.py:17
  1464.5 15.1 %convolution_convert_fusion = bf16[128,4096]{1,0:T(8,128)(2,1)} fusion(bf16[2752,4096]{1,0:T(8,128)(2,1)} %all-gather.23.cloned.1.call-done, bf16[128,2752]{0,1:T(8,128)(2,1)S(1)} %convolution_convert_fusion.2, f32[1,128,2752]{1,2,0:T(8,128)} %convert_bitcast_fusion, f32[1,128,2752]{1,2,0:T(8,128)} %convert_bitcast_fusion.1, ...), kind=kOutput, calls=%fused_computation | convolution fusion | flops 2914385920 | bytes 27908096 | tf_op jit(solution)/shard_map/dot_general | solution.py:120
  1479.7 22.2 %reduce-scatter.5.cloned.1.call-done = bf16[128,1024]{1,0:T(8,128)(2,1)} async-done(((bf16[128,4096]{1,0:T(8,128)(2,1)}), bf16[128,1024]{1,0:T(8,128)(2,1)}) %reduce-scatter.5.cloned.1.call-update) | async-done | bytes 262160 | tf_op jit(solution)/shard_map/reduce_scatter | solution.py:123
  1501.9 1.7 add_convert_fusion
  (61 shorter events, 7.0 us)
Async XLA Ops:
  6.5 19.1 %all-gather.9.cloned.1.call-start = ((), (), s32[]{:S(2)}) async-start(), calls=%async_computation.2 | async-start | bytes 1310720 | tf_op jit(solution)/shard_map/all_gather | solution.py:73
  7.3 2.1 copy-start.5
  7.3 101.2 %all-gather.13.cloned.1.call-start = ((), (), s32[]{:S(2)}) async-start(), calls=%async_computation.4 | async-start | bytes 5242880 | tf_op jit(solution)/shard_map/all_gather | solution.py:11
  8.0 100.4 %copy-start.11 = (f32[4096]{0:T(1024)S(1)}, f32[4096]{0:T(1024)}, u32[]{:S(2)}) copy-start(f32[4096]{0:T(1024)} %param.18) | copy-start | bytes 49156
  8.0 181.0 %all-gather.11.cloned.1.call-start = ((), (), s32[]{:S(2)}) async-start(), calls=%async_computation.3 | async-start | bytes 5242880 | tf_op jit(solution)/shard_map/all_gather | solution.py:11
  8.8 260.7 %all-gather.15.cloned.1.call-start = ((), (), s32[]{:S(2)}) async-start(), calls=%async_computation.5 | async-start | bytes 5242880 | tf_op jit(solution)/shard_map/all_gather | solution.py:17
  9.3 286.6 %reduce-scatter.3.cloned.1.call-start = ((), (), s32[]{:S(2)}) async-start(), calls=%async_computation.6 | async-start | bytes 1310720 | tf_op jit(solution)/shard_map/reduce_scatter | solution.py:101
  111.7 77.3 %copy-start.3 = (bf16[128,4096]{1,0:T(8,128)(2,1)S(1)}, bf16[128,4096]{1,0:T(8,128)(2,1)}, u32[]{:S(2)}) copy-start(bf16[128,4096]{1,0:T(8,128)(2,1)} %all-gather.9.cloned.1.call-done) | copy-start | bytes 3145732
  112.9 79.8 %copy-start.8 = (f32[4,128]{1,0:T(4,128)S(1)}, f32[4,128]{1,0:T(4,128)}, u32[]{:S(2)}) copy-start(f32[4,128]{1,0:T(4,128)} %param.23) | copy-start | bytes 6148
  112.9 79.8 %copy-start.9 = (f32[4,128]{1,0:T(4,128)S(1)}, f32[4,128]{1,0:T(4,128)}, u32[]{:S(2)}) copy-start(f32[4,128]{1,0:T(4,128)} %param.21) | copy-start | bytes 6148
  192.0 1.0 copy-start.10
  269.4 26.5 %copy-start.2 = (bf16[128,1024]{1,0:T(8,128)(2,1)S(1)}, bf16[128,1024]{1,0:T(8,128)(2,1)}, u32[]{:S(2)}) copy-start(bf16[128,1024]{1,0:T(8,128)(2,1)} %param.17) | copy-start | bytes 786436
  273.4 41.0 %all-gather.17.cloned.1.call-start = ((), (), s32[]{:S(2)}) async-start(), calls=%async_computation.7 | async-start | bytes 1310720 | tf_op jit(solution)/shard_map/all_gather | solution.py:105
  297.7 401.9 %all-gather.19.cloned.1.call-start = ((), (), s32[]{:S(2)}) async-start(), calls=%async_computation.8 | async-start | bytes 28180480 | tf_op jit(solution)/shard_map/all_gather | solution.py:11
  298.4 783.6 %all-gather.21.cloned.1.call-start = ((), (), s32[]{:S(2)}) async-start(), calls=%async_computation.9 | async-start | bytes 28180480 | tf_op jit(solution)/shard_map/all_gather | solution.py:11
  299.2 1.0 copy-start.6
  299.2 1.0 copy-start.7
  299.2 400.4 %copy-start.4 = (f32[4096]{0:T(1024)S(1)}, f32[4096]{0:T(1024)}, u32[]{:S(2)}) copy-start(f32[4096]{0:T(1024)} %param.26) | copy-start | bytes 49156
  299.2 1165.3 %all-gather.23.cloned.1.call-start = ((), (), s32[]{:S(2)}) async-start(), calls=%async_computation.10 | async-start | bytes 28180480 | tf_op jit(solution)/shard_map/all_gather | solution.py:17
  300.0 1201.9 %reduce-scatter.5.cloned.1.call-start = ((), (), s32[]{:S(2)}) async-start(), calls=%async_computation.11 | async-start | bytes 1310720 | tf_op jit(solution)/shard_map/reduce_scatter | solution.py:123
  314.4 385.1 %copy-start = (bf16[128,4096]{1,0:T(8,128)(2,1)S(1)}, bf16[128,4096]{1,0:T(8,128)(2,1)}, u32[]{:S(2)}) copy-start(bf16[128,4096]{1,0:T(8,128)(2,1)} %all-gather.17.cloned.1.call-done) | copy-start | bytes 3145732
  1094.0 370.6 %copy-start.12 = (f32[2752]{0:T(1024)S(1)}, f32[2752]{0:T(1024)}, u32[]{:S(2)}) copy-start(f32[2752]{0:T(1024)} %param.32) | copy-start | bytes 33028
  1094.0 370.6 %copy-start.13 = (f32[2752]{0:T(1024)S(1)}, f32[2752]{0:T(1024)}, u32[]{:S(2)}) copy-start(f32[2752]{0:T(1024)} %param.31) | copy-start | bytes 33028
  1464.5 37.4 %copy-start.1 = (bf16[128,1024]{1,0:T(8,128)(2,1)S(1)}, bf16[128,1024]{1,0:T(8,128)(2,1)}, u32[]{:S(2)}) copy-start(bf16[128,1024]{1,0:T(8,128)(2,1)} %add_convert_fusion.1) | copy-start | bytes 786436
Sparse Core Ops, SparseCore 0:
  8.9 16.6 all-gather.8
  27.2 81.2 all-gather.12
  110.0 78.9 all-gather.10
  190.4 78.9 all-gather.14
  273.5 22.3 reduce-scatter.2
  297.8 16.5 all-gather.16
  316.0 383.4 all-gather.18
  701.1 380.8 all-gather.20
  1083.6 380.8 all-gather.22
  1479.8 22.0 reduce-scatter.4
where the time goes:
time: 1510 us
  waiting for transfers between devices  1420 us (94%)
  matrix products  46.9 us (3%)
    all_gather x4, waiting for transfers between devices, gathered(): return lax.all_gather(part, axis, axis=dim, tiled=True)  913 us
    all_gather x2, waiting for transfers between devices, on_whole(): return work(lax.all_gather(shard, axis, axis=dim, tiled=True), jnp.int32(0))  446 us
  transfers between devices with their start and end apart: 10, of which 10 were waited for; matrix products, arithmetic and copies ran while one was open for 2% of the time, Pallas kernels for 0%

commit v1 on v0

v1 whole, which is shorter than its diff:
```python
import jax
import jax.numpy as jnp
from jax import lax
from jax.sharding import PartitionSpec as P

epsilon = 1e-06


def normalize(values, gain):
    values = values.astype(jnp.float32)
    scaled = values * lax.rsqrt(jnp.mean(values * values, axis=-1, keepdims=True) + epsilon)
    return scaled * gain


def gelu_exact(values):
    return jax.nn.gelu(values, approximate=False)


def convolve(values, kernel, offset, length):
    total_rows, width = values.shape
    blocks = values.reshape(total_rows // length, length, width)
    padded = jnp.pad(blocks, ((0, 0), (1, 1), (0, 0)))
    result = (
        offset
        + padded[:, 0:length] * kernel[0]
        + padded[:, 1 : length + 1] * kernel[1]
        + padded[:, 2:] * kernel[2]
    )
    return result.reshape(total_rows, width)


def dot(a, b):
    return jnp.dot(a, b, preferred_element_type=jnp.float32).astype(jnp.bfloat16)


def swap(block, fs, tp):
    if fs == tp:
        pairs = [(a * tp + b, b * tp + a) for a in range(fs) for b in range(tp)]
        return lax.ppermute(block, ("fs", "tp"), pairs)
    wide = lax.all_gather(block, "tp", axis=1, tiled=True)
    tall = lax.all_to_all(wide, "fs", 1, 0, tiled=True)
    rows = tall.shape[0] // tp
    return lax.dynamic_slice_in_dim(tall, lax.axis_index("tp") * rows, rows, 0)


def swap_back(block, fs, tp):
    if fs == tp:
        return swap(block, fs, tp)
    tall = lax.all_gather(block, "tp", axis=0, tiled=True)
    wide = lax.all_to_all(tall, "fs", 0, 1, tiled=True)
    columns = wide.shape[1] // tp
    return lax.dynamic_slice_in_dim(wide, lax.axis_index("tp") * columns, columns, 1)


def normed_rows(block, gain, fs):
    values = block.astype(jnp.float32)
    width = block.shape[1]
    square = lax.psum(jnp.sum(values * values, axis=1), "fs") / (width * fs)
    own = lax.dynamic_slice_in_dim(gain, lax.axis_index("fs") * width, width, 0)
    scaled = (values * lax.rsqrt(square + epsilon)[:, None] * own).astype(jnp.bfloat16)
    return lax.all_gather(scaled, "tp", axis=0, tiled=True)


def solution(mesh):
    fs, tp = mesh.shape["fs"], mesh.shape["tp"]

    def on_device(
        tokens,
        mixer_gain,
        gate_proj,
        value_proj,
        value_gain,
        spatial_mix,
        spatial_bias,
        head_gain,
        merge_proj,
        ffn_gain,
        gate_up,
        value_up,
        gate_kernel,
        value_kernel,
        gate_offset,
        value_offset,
        down_proj,
    ):
        heads_here = spatial_mix.shape[0]
        length = spatial_mix.shape[2]
        width = gate_proj.shape[1]
        head_width = width // heads_here
        rows = tokens.shape[0]
        seqs = rows // length
        matrix = lax.all_gather(spatial_mix, "fs", axis=1, tiled=True)

        turned = swap(tokens, fs, tp)
        normed = normed_rows(turned, mixer_gain, fs)
        both = jnp.concatenate([dot(normed, gate_proj), dot(normed, value_proj)], axis=1)
        both = lax.psum_scatter(both, "fs", scatter_dimension=0, tiled=True).astype(jnp.float32)
        gated = gelu_exact(both[:, :width])
        spread = gelu_exact(both[:, width:])
        spread = normalize(spread.reshape(seqs, length, heads_here, head_width), value_gain).astype(
            jnp.bfloat16
        )
        mixed = jnp.einsum("hij,njhd->nihd", matrix, spread, preferred_element_type=jnp.float32)
        mixed = mixed + spatial_bias.T[None, :, :, None]
        joined = gated.reshape(seqs, length, heads_here, head_width) * mixed
        merged = normalize(joined, head_gain).astype(jnp.bfloat16).reshape(rows, width)

        merged = lax.all_gather(merged, "fs", axis=0, tiled=True)
        branch = lax.psum_scatter(dot(merged, merge_proj), "tp", scatter_dimension=0, tiled=True)
        hidden = (turned.astype(jnp.float32) + branch.astype(jnp.float32)).astype(jnp.bfloat16)

        normed_ffn = normed_rows(hidden, ffn_gain, fs)
        upper_gate = lax.psum_scatter(dot(normed_ffn, gate_up), "fs", scatter_dimension=0, tiled=True)
        upper_value = lax.psum_scatter(dot(normed_ffn, value_up), "fs", scatter_dimension=0, tiled=True)
        conv_gate = convolve(upper_gate.astype(jnp.float32), gate_kernel, gate_offset, length)
        conv_value = convolve(upper_value.astype(jnp.float32), value_kernel, value_offset, length)
        active = (gelu_exact(conv_gate) * conv_value).astype(jnp.bfloat16)

        active = lax.all_gather(active, "fs", axis=0, tiled=True)
        change = lax.psum_scatter(dot(active, down_proj), "tp", scatter_dimension=0, tiled=True)
        result = (hidden.astype(jnp.float32) + change.astype(jnp.float32)).astype(jnp.bfloat16)
        return swap_back(result, fs, tp)

    in_specs = (
        P(("rep", "fs"), "tp"),
        P(),
        P("fs", "tp"),
        P("fs", "tp"),
        P("tp", None),
        P("tp", "fs", None),
        P("tp", None),
        P("tp", None),
        P("tp", "fs"),
        P(),
        P("fs", "tp"),
        P("fs", "tp"),
        P(None, "tp"),
        P(None, "tp"),
        P("tp"),
        P("tp"),
        P("tp", "fs"),
    )
    out_specs = P(("rep", "fs"), "tp")
    return jax.shard_map(
        on_device, mesh=mesh, in_specs=in_specs, out_specs=out_specs, check_vma=False
    )
```

time: 1510 us -> 407 us (0.27)
  waiting for transfers between devices: 1420 us -> 271 us
  blocking collectives: 13.6 us -> 51.1 us
  matrix products: 46.9 us -> 27.5 us
  local copies, waits for them, and re-layouts: 0.66 us -> 19 us
    all_gather x8 -> x3, waiting for transfers between devices: 1380 us -> 86.3 us  [the longest x1 57.5 us: on_device(): active = lax.all_gather(active, 'fs', axis=0, tiled=True)]
    unnamed x10 -> x11, waiting for transfers between devices: 4.73 us -> 114 us
    ppermute x0 -> x2, waiting for transfers between devices: none -> 25.5 us  [swap(): return lax.ppermute(block, ('fs', 'tp'), pairs)]
    psum x0 -> x2, blocking collectives: none -> 20.4 us  [normed_rows(): square = lax.psum(jnp.sum(values * values, axis=1), 'fs') / (width * fs)]
    dot_general x6, matrix products: 46.6 us -> 27.3 us  [dot(): jnp.dot(a, b, preferred_element_type=jnp.float32).astype(jnp.bfloat16)]
    unnamed x28 -> x35, local copies, waits for them, and re-layouts: 0.07 us -> 18.2 us
    all_gather x0 -> x1, blocking collectives: none -> 16.4 us  [on_device(): merged = lax.all_gather(merged, 'fs', axis=0, tiled=True)]
  transfers between devices with their start and end apart: 10 -> 10, of which waited for: 10 -> 10; matrix products, arithmetic and copies ran while one was open for 2% -> 4% of each run, Pallas kernels for 0% -> 0%
where the time goes in v1:
time: 407 us; the launch traced here: 406 us
  waiting for transfers between devices  271 us (67%)
  blocking collectives  51.1 us (13%)
  matrix products  27.5 us (7%)
  local copies, waits for them, and re-layouts  19 us (5%)
  between operations  13.7 us (3%)
  other arithmetic  13.5 us (3%)
  starting transfers between devices  10.5 us (3%)
    unnamed x11, waiting for transfers between devices  114 us
    all_gather x1, waiting for transfers between devices, on_device(): active = lax.all_gather(active, 'fs', axis=0, tiled=True)  57.5 us
    all_gather x2, waiting for transfers between devices, normed_rows(): return lax.all_gather(scaled, 'tp', axis=0, tiled=True)  28.8 us
    dot_general x6, matrix products, dot(): jnp.dot(a, b, preferred_element_type=jnp.float32).astype(jnp.bfloat16)  27.3 us
    ppermute x2, waiting for transfers between devices, swap(): return lax.ppermute(block, ('fs', 'tp'), pairs)  25.5 us
    reduce_scatter x1, waiting for transfers between devices, on_device(): lax.psum_scatter(dot(active, down_proj), 'tp', scatter_dimension=0, tiled...  22.9 us
    reduce_scatter x1, waiting for transfers between devices, on_device(): lax.psum_scatter(dot(merged, merge_proj), 'tp', scatter_dimension=0, tile...  21.8 us
    psum x2, blocking collectives, normed_rows(): square = lax.psum(jnp.sum(values * values, axis=1), 'fs') / (width * fs)  20.4 us
  transfers between devices with their start and end apart: 10, of which 10 were waited for; matrix products, arithmetic and copies ran while one was open for 4% of the time, Pallas kernels for 0%

profile of v1, /device:TPU:4, one launch (start us, length us, event | category | flops | bytes accessed | tf_op | source)
XLA Modules:
  0.0 406.2 jit_solution(7254583371773609787)
XLA Ops:
  6.5 4.6 %collective-permute-start = (bf16[128,1024]{1,0:T(8,128)(2,1)}, bf16[128,1024]{1,0:T(8,128)(2,1)S(1)}, u32[]{:S(2)}, u32[]{:S(2)}) collective-permute-start(bf16[128,1024]{1,0:T(8,128)(2,1)} %param.17), channel_id=1, source_target_pairs={{0,0},{1,4},{2,8},{3,12},{4,1},{5,5},{6,9},{7,13},{8,2},{9,6},{10,... | collective-permute-start | bytes 786440 | tf_op jit(solution)/shard_map/ppermute | solution.py:39
  11.8 12.9 %collective-permute-done = bf16[128,1024]{1,0:T(8,128)(2,1)S(1)} collective-permute-done((bf16[128,1024]{1,0:T(8,128)(2,1)}, bf16[128,1024]{1,0:T(8,128)(2,1)S(1)}, u32[]{:S(2)}, u32[]{:S(2)}) %collective-permute-start) | collective-permute-done | bytes 262176 | tf_op jit(solution)/shard_map/ppermute | solution.py:39
  24.8 8.5 %psum.14 = f32[128]{0:T(128)S(1)} all-reduce(f32[128]{0:T(128)S(1)} %fusion.34), channel_id=1, replica_groups=mesh['rep'=2,'fs'=4,'tp'=4] {'fs'}, use_global_device_ids=true, to_apply=%region_1.0 | all-reduce | flops 128 | bytes 1024 | tf_op jit(solution)/shard_map/psum | solution.py:58
  34.3 15.0 %all-gather.4.cloned.1.call-done = bf16[512,1024]{1,0:T(8,128)(2,1)} async-done(((bf16[128,1024]{1,0:T(8,128)(2,1)}), bf16[512,1024]{1,0:T(8,128)(2,1)}) %all-gather.4.cloned.1.call-update) | async-done | bytes 1048592 | tf_op jit(solution)/shard_map/all_gather | solution.py:61
  49.3 2.4 convolution_convert_fusion.4
  54.0 14.3 %all_gather.16 = bf16[4,128,128]{2,1,0:T(8,128)(2,1)S(1)} all-gather(bf16[4,32,128]{2,1,0:T(8,128)(2,1)S(1)} %copy-done.3), channel_id=1, replica_groups=mesh['rep'=2,'fs'=4,'tp'=4] {'fs'}, dimensions={1}, use_global_device_ids=true | all-gather | bytes 163840 | tf_op jit(solution)/shard_map/all_gather | solution.py:92
  68.3 15.1 %reduce-scatter.16.cloned.1.call-done = bf16[128,1024]{1,0:T(8,128)(2,1)} async-done(((bf16[512,1024]{1,0:T(8,128)(2,1)}), bf16[128,1024]{1,0:T(8,128)(2,1)}) %reduce-scatter.16.cloned.1.call-update) | async-done | bytes 262160
  86.2 16.4 %all_gather.17 = bf16[512,512]{0,1:T(8,128)(2,1)S(1)} all-gather(bf16[128,512]{0,1:T(8,128)(2,1)S(1)} %bitcast.125), channel_id=1, replica_groups=mesh['rep'=2,'fs'=4,'tp'=4] {'fs'}, dimensions={0}, use_global_device_ids=true | all-gather | bytes 655360 | tf_op jit(solution)/shard_map/all_gather | solution.py:108
  104.4 21.8 %reduce-scatter.12.cloned.1.call-done = bf16[128,1024]{1,0:T(8,128)(2,1)} async-done(((bf16[512,1024]{1,0:T(8,128)(2,1)}), bf16[128,1024]{1,0:T(8,128)(2,1)}) %reduce-scatter.12.cloned.1.call-update) | async-done | bytes 262160 | tf_op jit(solution)/shard_map/reduce_scatter | solution.py:109
  127.2 11.9 %psum.15 = f32[128]{0:T(128)S(1)} all-reduce(f32[128]{0:T(128)S(1)} %fusion.38), channel_id=1, replica_groups=mesh['rep'=2,'fs'=4,'tp'=4] {'fs'}, use_global_device_ids=true, to_apply=%region_7.0 | all-reduce | flops 128 | bytes 1024 | tf_op jit(solution)/shard_map/psum | solution.py:58
  139.1 1.8 fusion.40
  141.0 13.7 %all-gather.6.cloned.1.call-done = bf16[512,1024]{1,0:T(8,128)(2,1)} async-done(((bf16[128,1024]{1,0:T(8,128)(2,1)}), bf16[512,1024]{1,0:T(8,128)(2,1)}) %all-gather.6.cloned.1.call-update) | async-done | bytes 1048592 | tf_op jit(solution)/shard_map/all_gather | solution.py:61
  154.7 7.7 %convolution_convert_fusion = bf16[512,2752]{0,1:T(8,128)(2,1)} fusion(bf16[512,1024]{1,0:T(8,128)(2,1)} %all-gather.6.cloned.1.call-done, bf16[1024,2752]{0,1:T(8,128)(2,1)} %param.28), kind=kOutput, calls=%fused_computation | convolution fusion | flops 2887090176 | bytes 9502720 | tf_op jit(solution)/shard_map/dot_general | solution.py:33
  162.4 4.5 %copy.22 = bf16[512,2752]{1,0:T(8,128)(2,1)} copy(bf16[512,2752]{0,1:T(8,128)(2,1)} %convolution_convert_fusion) | data formatting | bytes 5636096
  168.2 7.1 %convolution_convert_fusion.1 = bf16[512,2752]{0,1:T(8,128)(2,1)} fusion(bf16[512,1024]{1,0:T(8,128)(2,1)S(1)} %copy-done.12, bf16[1024,2752]{0,1:T(8,128)(2,1)} %param.27), kind=kOutput, calls=%fused_computation.1 | convolution fusion | flops 2887090176 | bytes 9502720 | tf_op jit(solution)/shard_map/dot_general | solution.py:33
  175.3 4.5 %copy.20 = bf16[512,2752]{1,0:T(8,128)(2,1)} copy(bf16[512,2752]{0,1:T(8,128)(2,1)} %convolution_convert_fusion.1) | data formatting | bytes 5636096
  180.8 43.8 %reduce-scatter.20.cloned.1.call-done = bf16[128,2752]{1,0:T(8,128)(2,1)} async-done(((bf16[512,2752]{1,0:T(8,128)(2,1)}), bf16[128,2752]{1,0:T(8,128)(2,1)}) %reduce-scatter.20.cloned.1.call-update) | async-done | bytes 704528
  227.3 55.4 %reduce-scatter.18.cloned.1.call-done = bf16[128,2752]{1,0:T(8,128)(2,1)} async-done(((bf16[512,2752]{1,0:T(8,128)(2,1)}), bf16[128,2752]{1,0:T(8,128)(2,1)}) %reduce-scatter.18.cloned.1.call-update) | async-done | bytes 704528
  285.6 5.8 %fusion.8 = bf16[128,2752]{0,1:T(8,128)(2,1)} fusion(bf16[128,2752]{0,1:T(8,128)(2,1)S(1)} %copy.23, f32[1,128,2752]{1,2,0:T(8,128)S(1)} %copy-done.1, f32[1,128,2752]{1,2,0:T(8,128)S(1)} %convert_bitcast_fusion.1, bf16[128,2752]{0,1:T(8,128)(2,1)S(1)} %copy.21, f32[2752]{0:T(1024)S(1)} %get-tuple-element.9, f32[2752]{0:T(1024)S(1)} %get-tuple-element.10, ...), kind=kLoop, calls=%fused_computation.21 | loop fusion | flops 28180480 | bytes 5019648 | tf_op jit(solution)/shard_map/convert_element_type | solution.py:117
  291.5 57.5 %all-gather.8.cloned.1.call-done = bf16[512,2752]{0,1:T(8,128)(2,1)} async-done(((bf16[128,2752]{0,1:T(8,128)(2,1)}), bf16[512,2752]{0,1:T(8,128)(2,1)}) %all-gather.8.cloned.1.call-update) | async-done | bytes 2818064 | tf_op jit(solution)/shard_map/all_gather | solution.py:119
  349.0 7.6 %convolution_convert_fusion.2 = bf16[512,1024]{1,0:T(8,128)(2,1)} fusion(bf16[512,2752]{0,1:T(8,128)(2,1)} %all-gather.8.cloned.1.call-done, bf16[2752,1024]{1,0:T(8,128)(2,1)} %param.33), kind=kOutput, calls=%fused_computation.11 | convolution fusion | flops 2886205440 | bytes 9502720 | tf_op jit(solution)/shard_map/dot_general | solution.py:33
  356.7 22.9 %reduce-scatter.14.cloned.1.call-done = bf16[128,1024]{1,0:T(8,128)(2,1)} async-done(((bf16[512,1024]{1,0:T(8,128)(2,1)}), bf16[128,1024]{1,0:T(8,128)(2,1)}) %reduce-scatter.14.cloned.1.call-update) | async-done | bytes 262160 | tf_op jit(solution)/shard_map/reduce_scatter | solution.py:120
  380.6 5.4 %collective-permute-start.1 = (bf16[128,1024]{1,0:T(8,128)(2,1)S(1)}, bf16[128,1024]{1,0:T(8,128)(2,1)S(1)}, u32[]{:S(2)}, u32[]{:S(2)}) collective-permute-start(bf16[128,1024]{1,0:T(8,128)(2,1)S(1)} %fusion.41), channel_id=1, source_target_pairs={{0,0},{1,4},{2,8},{3,12},{4,1},{5,5},{6,9},{7,13},{8,2},{9,6},{10,... | collective-permute-start | bytes 786440 | tf_op jit(solution)/shard_map/ppermute | solution.py:39
  386.1 12.6 %collective-permute-done.1 = bf16[128,1024]{1,0:T(8,128)(2,1)S(1)} collective-permute-done((bf16[128,1024]{1,0:T(8,128)(2,1)S(1)}, bf16[128,1024]{1,0:T(8,128)(2,1)S(1)}, u32[]{:S(2)}, u32[]{:S(2)}) %collective-permute-start.1) | collective-permute-done | bytes 262176 | tf_op jit(solution)/shard_map/ppermute | solution.py:39
  (71 shorter events, 19.2 us)
Async XLA Ops:
  6.5 96.0 %copy-start = (bf16[512,1024]{1,0:T(8,128)(2,1)S(1)}, bf16[512,1024]{1,0:T(8,128)(2,1)}, u32[]{:S(2)}) copy-start(bf16[512,1024]{1,0:T(8,128)(2,1)} %param.25) | copy-start | bytes 3145732
  6.5 42.8 %all-gather.4.cloned.1.call-start = ((), (), s32[]{:S(2)}) async-start(), calls=%async_computation.5 | async-start | bytes 1310720 | tf_op jit(solution)/shard_map/all_gather | solution.py:61
  6.5 18.2 %collective-permute-start = (bf16[128,1024]{1,0:T(8,128)(2,1)}, bf16[128,1024]{1,0:T(8,128)(2,1)S(1)}, u32[]{:S(2)}, u32[]{:S(2)}) collective-permute-start(bf16[128,1024]{1,0:T(8,128)(2,1)} %param.17), channel_id=1, source_target_pairs={{0,0},{1,4},{2,8},{3,12},{4,1},{5,5},{6,9},{7,13},{8,2},{9,6},{10,... | collective-permute-start | bytes 786440 | tf_op jit(solution)/shard_map/ppermute | solution.py:39
  34.2 17.5 %copy-start.11 = (bf16[1024,512]{1,0:T(8,128)(2,1)S(1)}, bf16[1024,512]{1,0:T(8,128)(2,1)}, u32[]{:S(2)}) copy-start(bf16[1024,512]{1,0:T(8,128)(2,1)} %param.19) | copy-start | bytes 3145732
  34.2 49.1 %reduce-scatter.16.cloned.1.call-start = ((), (), s32[]{:S(2)}) async-start(), calls=%async_computation.10 | async-start | bytes 1310720
  49.3 2.4 copy-start.13
  52.6 1.4 copy-start.3
  53.9 31.8 %copy-start.8 = (f32[4,128]{1,0:T(4,128)S(1)}, f32[4,128]{1,0:T(4,128)}, u32[]{:S(2)}) copy-start(f32[4,128]{1,0:T(4,128)} %param.23) | copy-start | bytes 6148
  54.0 31.8 %copy-start.9 = (f32[4,128]{1,0:T(4,128)S(1)}, f32[4,128]{1,0:T(4,128)}, u32[]{:S(2)}) copy-start(f32[4,128]{1,0:T(4,128)} %param.21) | copy-start | bytes 6148
  54.0 72.1 %reduce-scatter.12.cloned.1.call-start = ((), (), s32[]{:S(2)}) async-start(), calls=%async_computation.6 | async-start | bytes 1310720 | tf_op jit(solution)/shard_map/reduce_scatter | solution.py:109
  84.5 1.5 copy-start.10
  104.3 34.9 %dynamic-slice-start = ((f32[4096]{0:T(1024)}, s32[]{:T(128)}), f32[1024]{0:T(1024)S(1)}, s32[]{:S(2)}) async-start(f32[4096]{0:T(1024)} %param.26, s32[]{:T(128)} %select_n.4), calls=%async_computation.13 | async-start | bytes 8704 | tf_op jit(solution)/shard_map/dynamic_slice | solution.py:59
  104.3 50.4 %all-gather.6.cloned.1.call-start = ((), (), s32[]{:S(2)}) async-start(), calls=%async_computation.7 | async-start | bytes 1310720 | tf_op jit(solution)/shard_map/all_gather | solution.py:61
  140.9 83.7 %reduce-scatter.20.cloned.1.call-start = ((), (), s32[]{:S(2)}) async-start(), calls=%async_computation.12 | async-start | bytes 3604480
  166.9 1.2 copy-start.12
  167.0 115.8 %reduce-scatter.18.cloned.1.call-start = ((), (), s32[]{:S(2)}) async-start(), calls=%async_computation.11 | async-start | bytes 3604480
  179.8 0.8 copy-start.5
  179.8 169.2 %all-gather.8.cloned.1.call-start = ((), (), s32[]{:S(2)}) async-start(), calls=%async_computation.8 | async-start | bytes 3522560 | tf_op jit(solution)/shard_map/all_gather | solution.py:119
  284.2 1.4 copy-start.1
  284.2 1.4 copy-start.6
  284.2 1.3 copy-start.7
  291.4 88.1 %copy-start.2 = (bf16[128,1024]{1,0:T(8,128)(2,1)S(1)}, bf16[128,1024]{1,0:T(8,128)(2,1)}, u32[]{:S(2)}) copy-start(bf16[128,1024]{1,0:T(8,128)(2,1)} %reduce-scatter.12.cloned.1.call-done) | copy-start | bytes 786436
  291.4 88.1 %reduce-scatter.14.cloned.1.call-start = ((), (), s32[]{:S(2)}) async-start(), calls=%async_computation.9 | async-start | bytes 1310720 | tf_op jit(solution)/shard_map/reduce_scatter | solution.py:120
  380.6 18.0 %collective-permute-start.1 = (bf16[128,1024]{1,0:T(8,128)(2,1)S(1)}, bf16[128,1024]{1,0:T(8,128)(2,1)S(1)}, u32[]{:S(2)}, u32[]{:S(2)}) collective-permute-start(bf16[128,1024]{1,0:T(8,128)(2,1)S(1)} %fusion.41), channel_id=1, source_target_pairs={{0,0},{1,4},{2,8},{3,12},{4,1},{5,5},{6,9},{7,13},{8,2},{9,6},{10,... | collective-permute-start | bytes 786440 | tf_op jit(solution)/shard_map/ppermute | solution.py:39
  (1 other events, 0.8 us)
Sparse Core Ops, SparseCore 0:
  34.3 14.9 all-gather.3
  54.1 29.2 reduce-scatter.15
  104.4 21.6 reduce-scatter.11
  141.1 13.6 all-gather.5
  167.1 57.4 reduce-scatter.19
  226.8 55.8 reduce-scatter.17
  291.5 57.4 all-gather.7
  356.8 22.7 reduce-scatter.13
